TPU v7x, 32 devices: a whole 2x2x4 slice. The times are simulated.
32 devices in a mesh: grp: 2 (over y), sp: 4 (over z), tp: 4 (over x, core).
Axes of the slice: x: 2, y: 2, z: 4, core: 2. Of those that a mesh axis runs over, the one named last changes fastest.
Arguments:
- receptance: bfloat16 [1024, 1024], P(('grp', 'sp'), 'tp'), parts along dimension 0, may hold values from -6 to 6
- head_keys: bfloat16 [1024, 1024], P(('grp', 'sp'), 'tp'), parts along dimension 0, may hold values from -6 to 6
- head_values: bfloat16 [1024, 1024], P(('grp', 'sp'), 'tp'), parts along dimension 0, may hold values from -6 to 6
- decay_logits: bfloat16 [1024, 1024], P(('grp', 'sp'), 'tp'), parts along dimension 0, may hold values from -13 to 0
- decay_boost: float32 [1024, 1024], P(('grp', 'sp'), 'tp'), parts along dimension 0, may hold values from -1.4 to 0
- correction_logits: bfloat16 [1024, 1024], P(('grp', 'sp'), 'tp'), parts along dimension 0, may hold values from -6 to 4
- gate_logits: bfloat16 [1024, 1024], P(('grp', 'sp'), 'tp'), parts along dimension 0, may hold values from -8 to 8
- head_norm_gain: float32 [1024], P('tp'), may hold values from 0.1 to 1.9
- output_weight: bfloat16 [1024, 2048], P('tp'), may hold values from -0.1875 to 0.1875
- residual: bfloat16 [1024, 2048], P(('grp', 'sp', 'tp')), parts along dimension 0, may hold values from -4 to 4
- expert_norm_gain: float32 [2048], replicated, may hold values from 0.1 to 1.9
- routes: int32 [1024, 2], P(('grp', 'sp', 'tp')), parts along dimension 0, may hold values from 0 to 3, all different within a row; in each aligned block of 32 rows (0 to 31, 32 to 63, ...) at most 32 rows name the same one
- routing_weight: float32 [1024, 2], P(('grp', 'sp', 'tp')), parts along dimension 0, may hold values from 0.1 to 1
- expert_gate_weight: bfloat16 [4, 2048, 3584], P('sp', None, 'tp'), may hold values from -0.125 to 0.125
- expert_up_weight: bfloat16 [4, 2048, 3584], P('sp', None, 'tp'), may hold values from -0.125 to 0.125
- expert_down_weight: bfloat16 [4, 3584, 2048], P('sp', 'tp'), may hold values from -0.09375 to 0.09375
Outputs:
- layer_out: bfloat16 [1024, 2048], P(('grp', 'sp', 'tp')), parts along dimension 0
There are 2 independent parts, one for each index of `grp`. A program takes and returns all parts, laid end to end along the dimension named above; an argument that names none is the same for every part. Nothing has to cross between parts.
Inputs may be any that keep to these rules, and one draw needn't show every extreme that they name: Each row names 2 different experts. Among the positions that one index of sp+tp holds in routes, no expert is named by more than 32 of them, and in every draw some expert is named by exactly 32 of them there.
All inputs are finite; a program needn't handle non-finite values.
Results may differ from a plain program's by a relative error of at most 0.017.
Values may be sent and summed in bfloat16 or wider, within the bound.
A program may use at most 64 MiB of HBM per device.

v0:
```python
from functools import partial

import jax
import jax.numpy as jnp
from jax import lax
from jax.sharding import PartitionSpec as P

HEAD = 64
TOP = 2
BLK = 32
TOK_DEV = 128


highest = lax.Precision.HIGHEST


def prefix(x, axis, combine, identity):
    size, index = (lax.axis_size(axis), lax.axis_index(axis))
    everything = jax.tree.map(
        lambda part, kind: lax.all_gather(part.astype(kind), axis), x, (jnp.bfloat16, jnp.bfloat16)
    )
    start = jax.tree.map(
        lambda part, zero: jnp.broadcast_to(jnp.asarray(zero, part.dtype), part.shape), x, identity
    )

    def hop(k, before):
        reached = k < index
        new = combine(
            before, jax.tree.map(lambda part, own: part[k].astype(own.dtype), everything, x)
        )
        return jax.tree.map(lambda a, b: jnp.where(reached, a, b), new, before)

    return lax.fori_loop(0, size, hop, start)


def into_block_rows(array):
    blocks = array.shape[0] // BLK
    heads_here = array.shape[1] // HEAD
    return array.astype(jnp.float32).reshape(blocks, BLK, heads_here, HEAD).transpose(2, 0, 1, 3)


def square_product(first, second):
    return jnp.einsum("hij,hjk->hik", first, second, precision=highest)


def join_later(earlier, later):
    trans_a, state_a = earlier
    trans_b, state_b = later
    return (square_product(trans_a, trans_b), square_product(state_a, trans_b) + state_b)


def advance(carry, item):
    prod_now, state_now = carry
    trans_here, local_here = item
    return (
        (square_product(prod_now, trans_here), square_product(state_now, trans_here) + local_here),
        (prod_now, state_now),
    )


def body(
    receptance,
    head_keys,
    head_values,
    decay_logits,
    decay_boost,
    correction_logits,
    gate_logits,
    head_norm_gain,
    output_weight,
    residual,
    expert_norm_gain,
    routes,
    routing_weight,
    expert_gate_weight,
    expert_up_weight,
    expert_down_weight,
):
    length_here = receptance.shape[0]
    width_here = receptance.shape[1]
    query = into_block_rows(receptance)
    keyed = into_block_rows(head_keys)
    valued = into_block_rows(head_values)
    heads_here = query.shape[0]
    unit = keyed * lax.rsqrt(jnp.sum(keyed * keyed, axis=-1, keepdims=True) + 1e-06)
    rate = jax.nn.sigmoid(into_block_rows(correction_logits))
    decay_logarithm = -jnp.exp(
        -jax.nn.softplus(-into_block_rows(decay_logits)) - 0.5
    ) + into_block_rows(decay_boost)
    remove = -unit
    insert = unit * rate
    upto = jnp.cumsum(decay_logarithm, axis=2)
    before = upto - decay_logarithm
    final_log = upto[:, :, -1:, :]
    remove_scaled = remove * jnp.exp(before)
    query_scaled = query * jnp.exp(upto)
    insert_scaled = insert * jnp.exp(-upto)
    key_scaled = keyed * jnp.exp(-upto)
    position = jnp.arange(BLK)
    strict = (position[:, None] > position[None, :]).astype(jnp.float32)
    inclusive = (position[:, None] >= position[None, :]).astype(jnp.float32)
    pairwise = partial(jnp.einsum, "hntc,hnsc->hnts", precision=highest)
    apply_rows = partial(jnp.einsum, "hnts,hnsc->hntc", precision=highest)
    outer_sum = partial(jnp.einsum, "hnsi,hnsj->hnij", precision=highest)
    among = pairwise(remove_scaled, insert_scaled) * strict
    among_keys = pairwise(remove_scaled, key_scaled) * strict
    read_insert = pairwise(query_scaled, insert_scaled) * inclusive
    read_keys = pairwise(query_scaled, key_scaled) * inclusive
    solver = jnp.eye(BLK, dtype=jnp.float32) + among
    power = among
    covered = 1
    while covered < BLK - 1:
        power = apply_rows(power, power)
        solver = solver + apply_rows(solver, power)
        covered = 2 * covered + 1
    from_start = apply_rows(solver, remove_scaled)
    from_local = apply_rows(solver, apply_rows(among_keys, valued))
    query_map = query_scaled + apply_rows(read_insert, from_start)
    local_out = apply_rows(read_insert, from_local) + apply_rows(read_keys, valued)
    tail = jnp.exp(final_log - upto)
    insert_tail = insert * tail
    key_tail = keyed * tail
    eye_head = jnp.eye(HEAD, dtype=jnp.float32)
    block_trans = eye_head * jnp.exp(final_log) + outer_sum(from_start, insert_tail)
    block_state = outer_sum(from_local, insert_tail) + outer_sum(valued, key_tail)
    start = (
        jnp.broadcast_to(eye_head, (heads_here, HEAD, HEAD)),
        jnp.zeros((heads_here, HEAD, HEAD), jnp.float32),
    )
    (device_trans, device_state), (prefix_trans, prefix_state) = lax.scan(
        advance, start, (block_trans.transpose(1, 0, 2, 3), block_state.transpose(1, 0, 2, 3))
    )
    carried_query = jnp.einsum("hntk,nhjk->hntj", query_map, prefix_trans, precision=highest)
    own_out = local_out + jnp.einsum("hntk,nhvk->hntv", query_map, prefix_state, precision=highest)
    incoming = prefix((device_trans, device_state), "sp", join_later, start)
    mixed = own_out + jnp.einsum("hntk,hvk->hntv", carried_query, incoming[1], precision=highest)
    centre = mixed - jnp.mean(mixed, axis=-1, keepdims=True)
    spread = jnp.mean(centre * centre, axis=-1, keepdims=True)
    normed = centre * lax.rsqrt(spread + 0.00064) * head_norm_gain.reshape(heads_here, 1, 1, HEAD)
    normed = normed.transpose(1, 2, 0, 3).reshape(length_here, width_here)
    gated = (normed * jax.nn.sigmoid(gate_logits.astype(jnp.float32))).astype(jnp.bfloat16)
    rows = gated
    branch = lax.psum_scatter(
        jnp.dot(rows, output_weight, preferred_element_type=jnp.float32).astype(jnp.bfloat16),
        "tp",
        scatter_dimension=0,
        tiled=True,
    ).astype(jnp.float32)
    stream = residual.astype(jnp.float32) + branch
    normal = (
        stream
        * lax.rsqrt(jnp.mean(stream * stream, axis=-1, keepdims=True) + 1e-06)
        * expert_norm_gain
    ).astype(jnp.bfloat16)
    sp_count = lax.axis_size("sp")
    tp_count = lax.axis_size("tp")
    capacity = max(2, 2 * TOK_DEV * TOP // (tp_count * sp_count))
    local_count = normal.shape[0]
    width_model = normal.shape[1]
    flat_routes = routes.reshape(-1)
    expert_ids = jnp.arange(sp_count, dtype=jnp.int32)
    chosen = (flat_routes[:, None] == expert_ids[None, :]).astype(jnp.int32)
    earlier = jnp.cumsum(chosen, axis=0) - chosen
    slot_index = jnp.sum(earlier * chosen, axis=1)
    target = flat_routes * capacity + slot_index
    placed = (target[:, None] == jnp.arange(sp_count * capacity, dtype=jnp.int32)[None, :]).astype(
        jnp.bfloat16
    )
    placed = jnp.sum(placed.reshape(local_count, TOP, sp_count * capacity), axis=1)
    outbound = jnp.einsum("ts,td->sd", placed, normal, preferred_element_type=jnp.float32).astype(
        jnp.bfloat16
    )
    outbound = outbound.reshape(sp_count, capacity, width_model)
    arrived = lax.all_to_all(outbound, "sp", split_axis=0, concat_axis=0, tiled=True)
    slots = arrived.shape[1]
    everyone = lax.all_gather(arrived[None], "tp", axis=0, tiled=True)
    rows = everyone.reshape(-1, width_model)
    hidden = (
        jax.nn.silu(jnp.dot(rows, expert_gate_weight[0], preferred_element_type=jnp.float32))
        * jnp.dot(rows, expert_up_weight[0], preferred_element_type=jnp.float32)
    ).astype(jnp.bfloat16)
    partial_rows = jnp.dot(
        hidden, expert_down_weight[0], preferred_element_type=jnp.float32
    ).reshape(tp_count, sp_count, slots, width_model)
    summed = lax.psum_scatter(
        partial_rows.astype(jnp.bfloat16), "tp", scatter_dimension=0, tiled=True
    ).astype(jnp.float32)
    summed = summed.astype(jnp.bfloat16).reshape(sp_count, slots, width_model)
    returned = lax.all_to_all(summed, "sp", split_axis=0, concat_axis=0, tiled=True)
    picked = returned.reshape(sp_count * capacity, width_model)[target].astype(jnp.float32)
    routed = jnp.sum(
        picked.reshape(local_count, TOP, width_model) * routing_weight[:, :, None], axis=1
    )
    return (stream + routed).astype(jnp.bfloat16)


def solution(mesh):
    placed = (
        P(("grp", "sp"), "tp"),
        P(("grp", "sp"), "tp"),
        P(("grp", "sp"), "tp"),
        P(("grp", "sp"), "tp"),
        P(("grp", "sp"), "tp"),
        P(("grp", "sp"), "tp"),
        P(("grp", "sp"), "tp"),
        P("tp"),
        P("tp", None),
        P(("grp", "sp", "tp"), None),
        P(),
        P(("grp", "sp", "tp"), None),
        P(("grp", "sp", "tp"), None),
        P("sp", None, "tp"),
        P("sp", None, "tp"),
        P("sp", "tp", None),
    )
    return jax.shard_map(
        body, mesh=mesh, in_specs=placed, out_specs=P(("grp", "sp", "tp"), None), check_vma=False
    )
```

profile of v0, /device:TPU:0, one launch (start us, length us, event | category | flops | bytes accessed | tf_op | source)
XLA Modules:
  0.0 209.4 jit_solution(14076337890120119313)
XLA Ops:
  6.6 1.1 reshape.161
  7.7 0.9 convert_negate_fusion
  8.7 1.0 reshape.174
  9.9 0.9 add_divide_fusion
  11.7 1.3 convolution_multiply_fusion.1
  13.0 0.6 convolution_multiply_fusion.2
  13.6 1.3 convolution_multiply_fusion.3
  14.9 1.3 convolution_multiply_fusion
  16.2 0.6 fusion.67
  17.6 0.4 convolution_add_fusion.3
  19.6 1.0 reshape.163
  21.4 1.3 fusion.52
  23.1 1.1 fusion.84
  24.1 1.1 convolution_add_fusion.6
  25.2 1.5 copy.82
  26.7 0.4 convolution_bitcast_fusion.3
  27.1 2.0 fusion.31
  29.1 1.1 fusion.32
  30.2 6.9 %while.31 = (s32[]{:T(128)}, f32[4,64,64]{1,2,0:T(8,128)S(1)}, f32[4,64,64]{1,2,0:T(8,128)S(1)}, f32[4,4,64,64]{2,3,0,1:T(8,128)}, f32[4,4,64,64]{2,3,0,1:T(8,12...) while((s32[]{:T(128)}, f32[4,64,64]{1,2,0:T(8,128)S(1)}, ...), condition=%wide.region_3.4_spmd.clone, body=%wide.region_2.3_spmd.clone.sunk | while | flops 25214980 | bytes 1704064 | solution.py:130
  30.3 0.7 bitcast_dynamic-update-slice_fusion.3
  31.6 0.4 fusion.139
  32.0 0.7 bitcast_dynamic-update-slice_fusion.3
  33.3 0.4 fusion.139
  33.7 0.8 bitcast_dynamic-update-slice_fusion.3
  35.0 0.4 fusion.139
  35.5 0.8 bitcast_dynamic-update-slice_fusion.3
  36.8 0.4 fusion.139
  37.3 15.7 %all-gather = bf16[16,64,64]{2,1,0:T(8,128)(2,1)S(1)} all-gather(bf16[4,64,64]{2,1,0:T(8,128)(2,1)S(1)} %copy.88), channel_id=2, replica_groups=mesh['grp'=2,'sp'=4,'tp'=4] {'sp'}, dimensions={0}, use_global_device_ids=true | all-gather | bytes 163840 | tf_op jit(solution)/shard_map/all_gather | solution.py:20
  53.1 14.8 %all-gather.1 = bf16[16,64,64]{2,1,0:T(8,128)(2,1)S(1)} all-gather(bf16[4,64,64]{2,1,0:T(8,128)(2,1)S(1)} %copy.89), channel_id=3, replica_groups=mesh['grp'=2,'sp'=4,'tp'=4] {'sp'}, dimensions={0}, use_global_device_ids=true | all-gather | bytes 163840 | tf_op jit(solution)/shard_map/all_gather | solution.py:20
  67.8 1.8 while.32
  70.0 0.6 fusion.86
  70.8 0.6 convolution_add_fusion.5
  71.4 0.5 fusion.78
  72.8 1.1 convolution_convert_fusion.1
  74.8 21.9 %reduce-scatter.3.cloned.1.call-done = bf16[32,2048]{1,0:T(8,128)(2,1)} async-done(((bf16[128,2048]{1,0:T(8,128)(2,1)}), bf16[32,2048]{1,0:T(8,128)(2,1)}) %reduce-scatter.3.cloned.1.call-update) | async-done | bytes 131088 | tf_op jit(solution)/shard_map/reduce_scatter | solution.py:143
  96.7 1.1 multiply_reduce_fusion.1
  97.8 1.2 convolution_convert_fusion
  99.0 18.8 %all_to_all.10 = bf16[4,32,2048]{2,1,0:T(8,128)(2,1)} all-to-all(bf16[4,32,2048]{2,1,0:T(8,128)(2,1)S(1)} %bitcast.205), channel_id=1, replica_groups=mesh['grp'=2,'sp'=4,'tp'=4] {'sp'}, dimensions={0} | all-to-all | bytes 1048576 | tf_op jit(solution)/shard_map/all_to_all | solution.py:174
  118.0 20.8 %all-gather.5.cloned.1.call-done = bf16[16,32,2048]{2,1,0:T(8,128)(2,1)} async-done(((bf16[4,32,2048]{2,1,0:T(8,128)(2,1)}), bf16[16,32,2048]{2,1,0:T(8,128)(2,1)}) %all-gather.5.cloned.1.call-update) | async-done | bytes 2097168 | tf_op jit(solution)/shard_map/all_gather | solution.py:176
  138.8 5.1 %fusion.24 = f32[512,896]{1,0:T(8,128)S(1)} fusion(bf16[512,2048]{1,0:T(8,128)(2,1)} %bitcast.213, bf16[1,2048,896]{2,1,0:T(8,128)(2,1)} %param.33), kind=kOutput, calls=%fused_computation.32 | convolution fusion | flops 1879048192 | bytes 7602176 | tf_op jit(solution)/shard_map/dot_general | solution.py:179
  143.9 2.4 %multiply_convert_fusion = bf16[512,896]{1,0:T(8,128)(2,1)S(1)} fusion(f32[512,896]{1,0:T(8,128)S(1)} %fusion.24, bf16[512,2048]{1,0:T(8,128)(2,1)S(1)} %bitcast.214, bf16[1,2048,896]{2,1,0:T(8,128)(2,1)S(1)} %copy-done.17), kind=kOutput, calls=%fused_computation.37 | convolution fusion | flops 1881800704 | bytes 8519680 | tf_op jit(solution)/shard_map/dot_general | solution.py:180
  146.4 3.7 %fusion.26 = bf16[4,4,32,2048]{3,2,1,0:T(8,128)(2,1)} fusion(bf16[4,4,32,896]{3,2,1,0:T(8,128)(2,1)S(1)} %bitcast.215, bf16[1,896,2048]{2,1,0:T(8,128)(2,1)S(1)} %copy-done.18), kind=kOutput, calls=%fused_computation.34 | convolution fusion | flops 1880096768 | bytes 6684672 | tf_op jit(solution)/shard_map/dot_general | solution.py:182
  150.1 31.3 %reduce-scatter.5.cloned.1.call-done = bf16[1,4,32,2048]{3,2,1,0:T(8,128)(2,1)} async-done(((bf16[4,4,32,2048]{3,2,1,0:T(8,128)(2,1)}), bf16[1,4,32,2048]{3,2,1,0:T(8,128)(2,1)}) %reduce-scatter.5.cloned.1.call-update) | async-done | bytes 524304 | tf_op jit(solution)/shard_map/reduce_scatter | solution.py:185
  181.4 4.6 %all-to-all-start.1 = ((bf16[4,32,2048]{2,1,0:T(8,128)(2,1)}), bf16[4,32,2048]{2,1,0:T(8,128)(2,1)S(1)}, u32[]{:S(2)}, u32[]{:S(2)}) async-start(bf16[4,32,2048]{2,1,0:T(8,128)(2,1)} %bitcast.208), calls=%async_computation.3 | async-start | bytes 1048576 | tf_op jit(solution)/shard_map/all_to_all | solution.py:189
  186.2 14.1 %all-to-all-done.1 = bf16[4,32,2048]{2,1,0:T(8,128)(2,1)S(1)} async-done(((bf16[4,32,2048]{2,1,0:T(8,128)(2,1)}), bf16[4,32,2048]{2,1,0:T(8,128)(2,1)S(1)}, u32[]{:S(2)}, u32[]{:S(2)}) %all-to-all-start.1) | async-done | bytes 524320 | tf_op jit(solution)/shard_map/all_to_all | solution.py:189
  200.3 0.7 gather_fusion
  201.4 0.7 multiply_reduce_fusion
  202.2 0.7 add_convert_fusion
  (133 shorter events, 11.5 us)
Async XLA Ops:
  6.5 66.3 %copy-start = (bf16[256,2048]{1,0:T(8,128)(2,1)S(1)}, bf16[256,2048]{1,0:T(8,128)(2,1)}, u32[]{:S(2)}) copy-start(bf16[256,2048]{1,0:T(8,128)(2,1)} %param.28) | copy-start | bytes 3145732
  6.5 4.4 %copy-start.12 = (bf16[128,256]{1,0:T(8,128)(2,1)S(1)}, bf16[128,256]{1,0:T(8,128)(2,1)}, u32[]{:S(2)}) copy-start(bf16[128,256]{1,0:T(8,128)(2,1)} %param.20) | copy-start | bytes 196612
  6.5 90.2 %reduce-scatter.3.cloned.1.call-start = ((), (), s32[]{:S(2)}) async-start(), calls=%async_computation.4 | async-start | bytes 655360 | tf_op jit(solution)/shard_map/reduce_scatter | solution.py:143
  19.2 3.9 %copy-start.2 = (f32[4,4,32,32]{3,2,1,0:T(8,128)S(1)}, f32[4,4,32,32]{3,2,1,0:T(8,128)}, u32[]{:S(2)}) copy-start(f32[4,4,32,32]{3,2,1,0:T(8,128)} %convolution_multiply_fusion.3) | copy-start | bytes 196612
  21.3 2.8 %copy-start.3 = (f32[4,4,32,64]{3,2,1,0:T(8,128)}, f32[4,4,32,64]{3,2,1,0:T(8,128)S(1)}, u32[]{:S(2)}) copy-start(f32[4,4,32,64]{3,2,1,0:T(8,128)S(1)} %fusion.85) | copy-start | bytes 393220
  26.7 3.5 %copy-start.10 = (f32[64,64]{0,1:T(8,128)S(1)}, f32[64,64]{0,1:T(8,128)}, u32[]{:S(2)}) copy-start(f32[64,64]{0,1:T(8,128)} %copy.82) | copy-start | bytes 49156
  53.0 16.6 %copy-start.14 = (f32[256]{0:T(256)S(1)}, f32[256]{0:T(256)}, u32[]{:S(2)}) copy-start(f32[256]{0:T(256)} %param.27) | copy-start | bytes 3076
  67.8 1.9 copy-start.6
  67.8 1.9 copy-start.7
  67.8 2.2 %copy-start.1 = (f32[4,4,32,64]{3,2,1,0:T(8,128)S(1)}, f32[4,4,32,64]{3,2,1,0:T(8,128)}, u32[]{:S(2)}) copy-start(f32[4,4,32,64]{3,2,1,0:T(8,128)} %convolution_add_fusion.6) | copy-start | bytes 393220
  67.8 2.2 %copy-start.8 = (f32[4,4,64,64]{2,3,0,1:T(8,128)S(1)}, f32[4,4,64,64]{2,3,0,1:T(8,128)}, u32[]{:S(2)}) copy-start(f32[4,4,64,64]{2,3,0,1:T(8,128)} %get-tuple-element.140) | copy-start | bytes 786436
  69.7 1.0 copy-start.9
  70.6 2.2 %copy-start.11 = (bf16[128,256]{1,0:T(8,128)(2,1)S(1)}, bf16[128,256]{1,0:T(8,128)(2,1)}, u32[]{:S(2)}) copy-start(bf16[128,256]{1,0:T(8,128)(2,1)} %param.26) | copy-start | bytes 196612
  71.9 2.1 %copy-start.15 = (s32[32,2]{0,1:T(2,128)S(1)}, s32[32,2]{0,1:T(2,128)}, u32[]{:S(2)}) copy-start(s32[32,2]{0,1:T(2,128)} %param.31) | copy-start | bytes 772
  71.9 24.8 %copy-start.4 = (bf16[32,2048]{1,0:T(8,128)(2,1)S(1)}, bf16[32,2048]{1,0:T(8,128)(2,1)}, u32[]{:S(2)}) copy-start(bf16[32,2048]{1,0:T(8,128)(2,1)} %param.29) | copy-start | bytes 393220
  72.2 25.6 %copy-start.13 = (f32[2048]{0:T(1024)S(1)}, f32[2048]{0:T(1024)}, u32[]{:S(2)}) copy-start(f32[2048]{0:T(1024)} %param.30) | copy-start | bytes 24580
  73.9 64.8 %all-gather.5.cloned.1.call-start = ((), (), s32[]{:S(2)}) async-start(), calls=%async_computation.6 | async-start | bytes 2621440 | tf_op jit(solution)/shard_map/all_gather | solution.py:176
  117.9 63.5 %reduce-scatter.5.cloned.1.call-start = ((), (), s32[]{:S(2)}) async-start(), calls=%async_computation.5 | async-start | bytes 2621440 | tf_op jit(solution)/shard_map/reduce_scatter | solution.py:185
  138.8 5.2 %copy-start.17 = (bf16[1,2048,896]{2,1,0:T(8,128)(2,1)S(1)}, bf16[1,2048,896]{2,1,0:T(8,128)(2,1)}, u32[]{:S(2)}) copy-start(bf16[1,2048,896]{2,1,0:T(8,128)(2,1)} %param.34) | copy-start | bytes 11010052
  138.8 5.2 %copy-start.19 = (bf16[16,32,2048]{2,1,0:T(8,128)(2,1)S(1)}, bf16[16,32,2048]{2,1,0:T(8,128)(2,1)}, u32[]{:S(2)}) copy-start(bf16[16,32,2048]{2,1,0:T(8,128)(2,1)} %all-gather.5.cloned.1.call-done) | copy-start | bytes 6291460
  143.9 2.4 %copy-start.18 = (bf16[1,896,2048]{2,1,0:T(8,128)(2,1)S(1)}, bf16[1,896,2048]{2,1,0:T(8,128)(2,1)}, u32[]{:S(2)}) copy-start(bf16[1,896,2048]{2,1,0:T(8,128)(2,1)} %param.35) | copy-start | bytes 11010052
  150.0 36.1 %copy-start.16 = (f32[32,2]{0,1:T(2,128)S(1)}, f32[32,2]{0,1:T(2,128)}, u32[]{:S(2)}) copy-start(f32[32,2]{0,1:T(2,128)} %param.32) | copy-start | bytes 772
  181.4 18.9 %all-to-all-start.1 = ((bf16[4,32,2048]{2,1,0:T(8,128)(2,1)}), bf16[4,32,2048]{2,1,0:T(8,128)(2,1)S(1)}, u32[]{:S(2)}, u32[]{:S(2)}) async-start(bf16[4,32,2048]{2,1,0:T(8,128)(2,1)} %bitcast.208), calls=%async_computation.3 | async-start | bytes 1048576 | tf_op jit(solution)/shard_map/all_to_all | solution.py:189
  186.0 16.1 %copy-start.5 = (bf16[32,2048]{1,0:T(8,128)(2,1)S(1)}, bf16[32,2048]{1,0:T(8,128)(2,1)}, u32[]{:S(2)}) copy-start(bf16[32,2048]{1,0:T(8,128)(2,1)} %reduce-scatter.3.cloned.1.call-done) | copy-start | bytes 393220
Sparse Core Ops, SparseCore 0:
  74.1 22.5 reduce-scatter.2
  118.0 20.6 all-gather.4
  150.2 31.1 reduce-scatter.4
where the time goes:
time: 210 us; the launch traced here: 209 us
  waiting for transfers between devices  88.2 us (42%)
  blocking collectives  49.3 us (23%)
  matrix products  35 us (17%)
  between operations  13.7 us (7%)
  other arithmetic  9.57 us (5%)
  local copies, waits for them, and re-layouts  8.63 us (4%)
  starting transfers between devices  4.68 us (2%)
    reduce_scatter x1, waiting for transfers between devices, body(): lax.psum_scatter(partial_rows.astype(jnp.bfloat16), 'tp', scatter_dimensi...  31.3 us
    all_gather x2, blocking collectives, prefix(): lax.all_gather(part.astype(kind), axis)  30.4 us
    reduce_scatter x1, waiting for transfers between devices, body(): lax.psum_scatter(jnp.dot(rows, output_weight, preferred_element_type=jnp....  21.9 us
    all_gather x1, waiting for transfers between devices, body(): everyone = lax.all_gather(arrived[None], 'tp', axis=0, tiled=True)  20.8 us
    all_to_all x1, blocking collectives, body(): lax.all_to_all(outbound, 'sp', split_axis=0, concat_axis=0, tiled=True)  18.8 us
    all_to_all x1, waiting for transfers between devices, body(): lax.all_to_all(summed, 'sp', split_axis=0, concat_axis=0, tiled=True)  14.1 us
    dot_general x1, matrix products, body(): jnp.dot(rows, expert_gate_weight[0], preferred_element_type=jnp.float32)  5.14 us
    all_to_all x1, starting transfers between devices, body(): lax.all_to_all(summed, 'sp', split_axis=0, concat_axis=0, tiled=True)  4.6 us
  transfers between devices with their start and end apart: 4, of which 4 were waited for; matrix products, arithmetic and copies ran while one was open for 0% of the time, Pallas kernels for 0%

commit v1 on v0

--- a/solution.py
+++ b/solution.py
@@ -3,6 +3,8 @@
 import jax
 import jax.numpy as jnp
 from jax import lax
+from jax.experimental import pallas as pl
+from jax.experimental.pallas import tpu as pltpu
 from jax.sharding import PartitionSpec as P
 
 HEAD = 64
@@ -14,23 +16,418 @@
 highest = lax.Precision.HIGHEST
 
 
+MESH = pl.DeviceIdType.MESH
+
+
+def share_kernel(size, own_ref, all_ref, send_sem, recv_sem):
+    me = lax.axis_index("sp")
+    barrier = pltpu.get_barrier_semaphore()
+    for k in range(1, size):
+        peer = lax.rem(me + k, size)
+        pl.semaphore_signal(barrier, inc=1, device_id={"sp": peer}, device_id_type=MESH)
+    pl.semaphore_wait(barrier, size - 1)
+
+    def transfer(slot, peer):
+        return pltpu.make_async_remote_copy(
+            src_ref=own_ref,
+            dst_ref=all_ref.at[slot],
+            send_sem=send_sem.at[peer],
+            recv_sem=recv_sem.at[slot],
+            device_id={"sp": peer},
+            device_id_type=MESH,
+        )
+
+    def each(action):
+        def step(peer, carry):
+            action(peer)
+            return carry
+
+        lax.fori_loop(0, size, step, 0)
+
+    def send(peer):
+        @pl.when(peer > me)
+        def _():
+            transfer(me, peer).start()
+
+        @pl.when(peer >= me)
+        def _():
+            all_ref[peer] = jnp.zeros(own_ref.shape, own_ref.dtype)
+
+    def finish(peer):
+        @pl.when(peer > me)
+        def _():
+            transfer(me, peer).wait_send()
+
+        @pl.when(peer < me)
+        def _():
+            transfer(peer, peer).wait_recv()
+
+    each(send)
+    each(finish)
+
+
 def prefix(x, axis, combine, identity):
     size, index = (lax.axis_size(axis), lax.axis_index(axis))
-    everything = jax.tree.map(
-        lambda part, kind: lax.all_gather(part.astype(kind), axis), x, (jnp.bfloat16, jnp.bfloat16)
-    )
-    start = jax.tree.map(
-        lambda part, zero: jnp.broadcast_to(jnp.asarray(zero, part.dtype), part.shape), x, identity
-    )
-
-    def hop(k, before):
-        reached = k < index
-        new = combine(
-            before, jax.tree.map(lambda part, own: part[k].astype(own.dtype), everything, x)
-        )
-        return jax.tree.map(lambda a, b: jnp.where(reached, a, b), new, before)
-
-    return lax.fori_loop(0, size, hop, start)
+    own = jnp.concatenate([part.astype(jnp.bfloat16) for part in x], axis=-1)
+    everything = pl.pallas_call(
+        partial(share_kernel, size),
+        out_shape=jax.ShapeDtypeStruct((size,) + own.shape, own.dtype),
+        in_specs=[pl.BlockSpec(memory_space=pltpu.VMEM)],
+        out_specs=pl.BlockSpec(memory_space=pltpu.VMEM),
+        scratch_shapes=[pltpu.SemaphoreType.DMA((size,)), pltpu.SemaphoreType.DMA((size,))],
+        compiler_params=pltpu.CompilerParams(collective_id=1, has_side_effects=True),
+    )(own)
+    before = identity
+    for k in range(size):
+        item = (
+            everything[k, :, :, :HEAD].astype(jnp.float32),
+            everything[k, :, :, HEAD:].astype(jnp.float32),
+        )
+        new = combine(before, item)
+        before = jax.tree.map(lambda p, q: jnp.where(k < index, p, q), new, before)
+    return before
+
+
+def tail_kernel(
+    sp_count,
+    tp_count,
+    cap,
+    gated_ref,
+    out_weight_ref,
+    residual_ref,
+    gain_ref,
+    place_ref,
+    combine_ref,
+    gate_hbm,
+    up_hbm,
+    down_hbm,
+    result_ref,
+    gate_ref,
+    up_ref,
+    down_ref,
+    part,
+    part_in,
+    stream_ref,
+    outbound,
+    rows,
+    partial_ref,
+    pair_in,
+    cross_out,
+    cross_in,
+    final_ref,
+    returned,
+    weight_sem,
+    part_send,
+    part_recv,
+    out_send,
+    out_recv,
+    fan_send,
+    row_recv,
+    pair_send,
+    pair_recv,
+    cross_send,
+    cross_recv,
+    final_send,
+    final_recv,
+):
+    sp, tp = lax.axis_index("sp"), lax.axis_index("tp")
+    chips = tp_count // 2
+    chip, core = tp // 2, lax.rem(tp, 2)
+    partner = chip * 2 + 1 - core
+    local = residual_ref.shape[0]
+    f32, bf16 = jnp.float32, jnp.bfloat16
+
+    weights = [
+        pltpu.make_async_copy(source.at[0], target, weight_sem.at[n])
+        for n, (source, target) in enumerate(
+            ((gate_hbm, gate_ref), (up_hbm, up_ref), (down_hbm, down_ref))
+        )
+    ]
+    for copy in weights:
+        copy.start()
+
+    barrier = pltpu.get_barrier_semaphore()
+    for k in range(1, sp_count):
+        peer = lax.rem(sp + k, sp_count)
+        pl.semaphore_signal(barrier, inc=1, device_id={"sp": peer}, device_id_type=MESH)
+    for k in range(1, tp_count):
+        peer = lax.rem(tp + k, tp_count)
+        pl.semaphore_signal(barrier, inc=1, device_id={"tp": peer}, device_id_type=MESH)
+    pl.semaphore_wait(barrier, sp_count + tp_count - 2)
+
+    def remote(source, target, send, recv, where):
+        return pltpu.make_async_remote_copy(
+            src_ref=source,
+            dst_ref=target,
+            send_sem=send,
+            recv_sem=recv,
+            device_id=where,
+            device_id_type=MESH,
+        )
+
+    def loop(count, action):
+        def step(k, carry):
+            action(k)
+            return carry
+
+        lax.fori_loop(0, count, step, 0)
+
+    def part_copy(slot, peer):
+        return remote(
+            part.at[peer], part_in.at[slot], part_send.at[peer], part_recv.at[slot], {"tp": peer}
+        )
+
+    for k in range(1, tp_count + 1):
+        peer = lax.rem(tp + k, tp_count)
+        piece = gated_ref[pl.ds(pl.multiple_of(peer * local, local), local), :]
+        part[peer] = jnp.dot(piece, out_weight_ref[...], preferred_element_type=f32).astype(bf16)
+        if k < tp_count:
+            part_copy(tp, peer).start()
+    stream = residual_ref[...].astype(f32) + part[tp].astype(f32)
+    for k in range(1, tp_count):
+        peer = lax.rem(tp + tp_count - k, tp_count)
+        part_copy(peer, peer).wait_recv()
+        stream = stream + part_in[peer].astype(f32)
+    stream_ref[...] = stream
+    normal = (
+        stream
+        * lax.rsqrt(jnp.mean(stream * stream, axis=-1, keepdims=True) + 1e-06)
+        * gain_ref[...]
+    ).astype(bf16)
+    sent = jnp.dot(place_ref[...], normal, preferred_element_type=f32).astype(bf16)
+    outbound[...] = sent.reshape(outbound.shape)
+
+    def block(ref, s, t):
+        return ref.at[s, pl.ds(pl.multiple_of(t * cap, cap), cap)]
+
+    def out_copy(slot, peer):
+        return remote(
+            outbound.at[peer],
+            block(rows, slot, tp),
+            out_send.at[peer],
+            out_recv.at[slot],
+            {"sp": peer},
+        )
+
+    def own_block(s):
+        return block(rows, s, tp)
+
+    def fan_copy(s, t, peer, slot):
+        return remote(
+            block(rows, s, t),
+            block(rows, s, t),
+            fan_send.at[s, slot],
+            row_recv.at[s, t],
+            {"tp": peer},
+        )
+
+    rows[sp, pl.ds(pl.multiple_of(tp * cap, cap), cap), :] = outbound[sp]
+
+    def dispatch(k):
+        out_copy(sp, lax.rem(sp + sp_count - k - 1, sp_count)).start()
+
+    loop(sp_count - 1, dispatch)
+
+    def at(k):
+        return lax.rem(sp + k, sp_count)
+
+    def counterpart(d):
+        return lax.rem(chip + d, chips) * 2 + core
+
+    def fan_first(k):
+        s = at(k)
+
+        @pl.when(k > 0)
+        def _():
+            out_copy(s, s).wait_recv()
+
+        for d in range(1, chips):
+            fan_copy(s, tp, counterpart(d), d - 1).start()
+        fan_copy(s, tp, partner, chips - 1).start()
+
+    def fan_second(k):
+        s = at(k)
+        for d in range(1, chips):
+            source = counterpart(chips - d)
+            fan_copy(s, source, source, 0).wait_recv()
+            fan_copy(s, source, partner, chips - 1 + d).start()
+
+    def pair_copy(s, a):
+        return remote(
+            block(partial_ref, s, a * 2 + 1 - core),
+            pair_in.at[s, a],
+            pair_send.at[s, a],
+            pair_recv.at[s, a],
+            {"tp": partner},
+        )
+
+    def cross_copy(s, a, slot):
+        return remote(
+            cross_out.at[s, a],
+            cross_in.at[s, slot],
+            cross_send.at[s, a],
+            cross_recv.at[s, slot],
+            {"tp": a * 2 + core},
+        )
+
+    def final_copy(s, slot):
+        return remote(
+            final_ref.at[s], returned.at[slot], final_send.at[s], final_recv.at[slot], {"sp": s}
+        )
+
+    def compute(k):
+        s = at(k)
+        for a in range(chips):
+            t = a * 2 + 1 - core
+            fan_copy(s, t, partner, 0).wait_recv()
+
+        @pl.when(k == 0)
+        def _():
+            for copy in weights:
+                copy.wait()
+
+        x = rows[s]
+        gate = jnp.dot(x, gate_ref[...], preferred_element_type=f32)
+        up = jnp.dot(x, up_ref[...], preferred_element_type=f32)
+        hidden = (gate / (1.0 + jnp.exp(-gate)) * up).astype(bf16)
+        partial_ref[s] = jnp.dot(hidden, down_ref[...], preferred_element_type=f32).astype(bf16)
+        for a in range(chips):
+            pair_copy(s, a).start()
+
+    def mine(s, a):
+        t = a * 2 + core
+        return partial_ref[s, pl.ds(pl.multiple_of(t * cap, cap), cap), :].astype(f32)
+
+    def cross(k):
+        s = at(k)
+        for d in range(1, chips):
+            a = lax.rem(chip + d, chips)
+            pair_copy(s, a).wait_recv()
+            cross_out[s, a] = (mine(s, a) + pair_in[s, a].astype(f32)).astype(bf16)
+            cross_copy(s, a, chip).start()
+
+    def finish(k):
+        s = at(k)
+        pair_copy(s, chip).wait_recv()
+        total = mine(s, chip) + pair_in[s, chip].astype(f32)
+        for d in range(1, chips):
+            a = lax.rem(chip + d, chips)
+            cross_copy(s, a, a).wait_recv()
+            total = total + cross_in[s, a].astype(f32)
+        final_ref[s] = total.astype(bf16)
+
+        @pl.when(k > 0)
+        def _():
+            final_copy(s, sp).start()
+
+    fan_first(0)
+    if sp_count > 1:
+        fan_first(1)
+    fan_second(0)
+
+    def turn(i):
+        @pl.when(i + 1 < sp_count)
+        def _():
+            fan_second(i + 1)
+
+        @pl.when(i < sp_count)
+        def _():
+            compute(i)
+
+        @pl.when(i + 2 < sp_count)
+        def _():
+            fan_first(i + 2)
+
+        @pl.when((i >= 1) & (i < sp_count + 1))
+        def _():
+            cross(i - 1)
+
+        @pl.when(i >= 2)
+        def _():
+            finish(i - 2)
+
+    loop(sp_count + 2, turn)
+
+    returned[sp] = final_ref[sp]
+
+    def collect(k):
+        s = lax.rem(sp + sp_count - k - 1, sp_count)
+        final_copy(s, s).wait_recv()
+
+    loop(sp_count - 1, collect)
+    picked = returned[...].reshape(sp_count * cap, returned.shape[2]).astype(f32)
+    routed = jnp.dot(combine_ref[...], picked, precision=highest, preferred_element_type=f32)
+    result_ref[...] = (stream_ref[...] + routed).astype(bf16)
+
+    for k in range(1, tp_count):
+        part_copy(tp, lax.rem(tp + k, tp_count)).wait_send()
+
+    def drain(k):
+        s = at(k)
+
+        @pl.when(k > 0)
+        def _():
+            out_copy(sp, s).wait_send()
+            final_copy(s, sp).wait_send()
+
+        for d in range(1, chips):
+            fan_copy(s, tp, counterpart(d), d - 1).wait_send()
+            fan_copy(s, counterpart(chips - d), partner, chips - 1 + d).wait_send()
+            a = lax.rem(chip + d, chips)
+            cross_copy(s, a, chip).wait_send()
+        fan_copy(s, tp, partner, chips - 1).wait_send()
+        for a in range(chips):
+            pair_copy(s, a).wait_send()
+
+    loop(sp_count, drain)
+
+
+def after_mixer(gated, out_weight, residual, gain, place, combine, gate_w, up_w, down_w, cap):
+    sp_count, tp_count = lax.axis_size("sp"), lax.axis_size("tp")
+    chips = tp_count // 2
+    local, width = residual.shape
+    bf16 = jnp.bfloat16
+    vmem = pl.BlockSpec(memory_space=pltpu.VMEM)
+    hbm = pl.BlockSpec(memory_space=pl.ANY)
+    dma = pltpu.SemaphoreType.DMA
+    return pl.pallas_call(
+        partial(tail_kernel, sp_count, tp_count, cap),
+        out_shape=jax.ShapeDtypeStruct((local, width), bf16),
+        in_specs=[vmem] * 6 + [hbm] * 3,
+        out_specs=vmem,
+        scratch_shapes=[
+            pltpu.VMEM(gate_w.shape[1:], bf16),
+            pltpu.VMEM(up_w.shape[1:], bf16),
+            pltpu.VMEM(down_w.shape[1:], bf16),
+            pltpu.VMEM((tp_count, local, width), bf16),
+            pltpu.VMEM((tp_count, local, width), bf16),
+            pltpu.VMEM((local, width), jnp.float32),
+            pltpu.VMEM((sp_count, cap, width), bf16),
+            pltpu.VMEM((sp_count, tp_count * cap, width), bf16),
+            pltpu.VMEM((sp_count, tp_count * cap, width), bf16),
+            pltpu.VMEM((sp_count, chips, cap, width), bf16),
+            pltpu.VMEM((sp_count, chips, cap, width), bf16),
+            pltpu.VMEM((sp_count, chips, cap, width), bf16),
+            pltpu.VMEM((sp_count, cap, width), bf16),
+            pltpu.VMEM((sp_count, cap, width), bf16),
+            dma((3,)),
+            dma((tp_count,)),
+            dma((tp_count,)),
+            dma((sp_count,)),
+            dma((sp_count,)),
+            dma((sp_count, tp_count)),
+            dma((sp_count, tp_count)),
+            dma((sp_count, chips)),
+            dma((sp_count, chips)),
+            dma((sp_count, chips)),
+            dma((sp_count, chips)),
+            dma((sp_count,)),
+            dma((sp_count,)),
+        ],
+        compiler_params=pltpu.CompilerParams(
+            collective_id=0, has_side_effects=True, vmem_limit_bytes=60 * 1024 * 1024
+        ),
+    )(gated, out_weight, residual, gain, place, combine, gate_w, up_w, down_w)
 
 
 def into_block_rows(array):
@@ -139,59 +536,34 @@
     normed = centre * lax.rsqrt(spread + 0.00064) * head_norm_gain.reshape(heads_here, 1, 1, HEAD)
     normed = normed.transpose(1, 2, 0, 3).reshape(length_here, width_here)
     gated = (normed * jax.nn.sigmoid(gate_logits.astype(jnp.float32))).astype(jnp.bfloat16)
-    rows = gated
-    branch = lax.psum_scatter(
-        jnp.dot(rows, output_weight, preferred_element_type=jnp.float32).astype(jnp.bfloat16),
-        "tp",
-        scatter_dimension=0,
-        tiled=True,
-    ).astype(jnp.float32)
-    stream = residual.astype(jnp.float32) + branch
-    normal = (
-        stream
-        * lax.rsqrt(jnp.mean(stream * stream, axis=-1, keepdims=True) + 1e-06)
-        * expert_norm_gain
-    ).astype(jnp.bfloat16)
     sp_count = lax.axis_size("sp")
     tp_count = lax.axis_size("tp")
     capacity = max(2, 2 * TOK_DEV * TOP // (tp_count * sp_count))
-    local_count = normal.shape[0]
-    width_model = normal.shape[1]
+    cap = -(-capacity // 16) * 16
+    local_count = residual.shape[0]
     flat_routes = routes.reshape(-1)
     expert_ids = jnp.arange(sp_count, dtype=jnp.int32)
     chosen = (flat_routes[:, None] == expert_ids[None, :]).astype(jnp.int32)
     earlier = jnp.cumsum(chosen, axis=0) - chosen
     slot_index = jnp.sum(earlier * chosen, axis=1)
-    target = flat_routes * capacity + slot_index
-    placed = (target[:, None] == jnp.arange(sp_count * capacity, dtype=jnp.int32)[None, :]).astype(
-        jnp.bfloat16
+    target = flat_routes * cap + slot_index
+    slots = jnp.arange(sp_count * cap, dtype=jnp.int32)
+    placed = (target[:, None] == slots[None, :]).reshape(local_count, TOP, sp_count * cap)
+    placed = placed.astype(jnp.float32)
+    place = jnp.sum(placed, axis=1).astype(jnp.bfloat16).T
+    combine = jnp.sum(placed * routing_weight[:, :, None], axis=1)
+    return after_mixer(
+        gated,
+        output_weight,
+        residual,
+        expert_norm_gain[None, :],
+        place,
+        combine,
+        expert_gate_weight,
+        expert_up_weight,
+        expert_down_weight,
+        cap,
     )
-    placed = jnp.sum(placed.reshape(local_count, TOP, sp_count * capacity), axis=1)
-    outbound = jnp.einsum("ts,td->sd", placed, normal, preferred_element_type=jnp.float32).astype(
-        jnp.bfloat16
-    )
-    outbound = outbound.reshape(sp_count, capacity, width_model)
-    arrived = lax.all_to_all(outbound, "sp", split_axis=0, concat_axis=0, tiled=True)
-    slots = arrived.shape[1]
-    everyone = lax.all_gather(arrived[None], "tp", axis=0, tiled=True)
-    rows = everyone.reshape(-1, width_model)
-    hidden = (
-        jax.nn.silu(jnp.dot(rows, expert_gate_weight[0], preferred_element_type=jnp.float32))
-        * jnp.dot(rows, expert_up_weight[0], preferred_element_type=jnp.float32)
-    ).astype(jnp.bfloat16)
-    partial_rows = jnp.dot(
-        hidden, expert_down_weight[0], preferred_element_type=jnp.float32
-    ).reshape(tp_count, sp_count, slots, width_model)
-    summed = lax.psum_scatter(
-        partial_rows.astype(jnp.bfloat16), "tp", scatter_dimension=0, tiled=True
-    ).astype(jnp.float32)
-    summed = summed.astype(jnp.bfloat16).reshape(sp_count, slots, width_model)
-    returned = lax.all_to_all(summed, "sp", split_axis=0, concat_axis=0, tiled=True)
-    picked = returned.reshape(sp_count * capacity, width_model)[target].astype(jnp.float32)
-    routed = jnp.sum(
-        picked.reshape(local_count, TOP, width_model) * routing_weight[:, :, None], axis=1
-    )
-    return (stream + routed).astype(jnp.bfloat16)
 
 
 def solution(mesh):

time: 210 us -> 103 us (0.49)
  waiting for transfers between devices: 88.2 us -> 0 us
  Pallas kernels: 0 us -> 66.3 us
  blocking collectives: 49.3 us -> 0 us
  matrix products: 35 us -> 20.3 us
  between operations: 13.7 us -> 0.49 us
  starting transfers between devices: 4.68 us -> 0 us
    pallas_call x0 -> x2, Pallas kernels: none -> 66.3 us  [the longest x1 55.5 us: after_mixer(): pl.pallas_call(partial(tail_kernel, sp_count, tp_count, cap), out_shape=j...]
    reduce_scatter x2 -> x0, waiting for transfers between devices: 53.2 us -> none  [the longest x1 31.3 us: body(): lax.psum_scatter(partial_rows.astype(jnp.bfloat16), 'tp', scatter_dimensi...]
    all_gather x2 -> x0, blocking collectives: 30.4 us -> none  [prefix(): lax.all_gather(part.astype(kind), axis)]
    all_gather x1 -> x0, waiting for transfers between devices: 20.8 us -> none  [body(): everyone = lax.all_gather(arrived[None], 'tp', axis=0, tiled=True)]
    all_to_all x1 -> x0, blocking collectives: 18.8 us -> none  [body(): lax.all_to_all(outbound, 'sp', split_axis=0, concat_axis=0, tiled=True)]
    all_to_all x1 -> x0, waiting for transfers between devices: 14.1 us -> none  [body(): lax.all_to_all(summed, 'sp', split_axis=0, concat_axis=0, tiled=True)]
    dot_general x5 -> x0, matrix products: 13.6 us -> none  [the longest x1 5.14 us: body(): jnp.dot(rows, expert_gate_weight[0], preferred_element_type=jnp.float32)]
    all_to_all x1 -> x0, starting transfers between devices: 4.6 us -> none  [body(): lax.all_to_all(summed, 'sp', split_axis=0, concat_axis=0, tiled=True)]
  transfers between devices with their start and end apart: 4 -> 0, of which waited for: 4 -> 0; matrix products, arithmetic and copies ran while one was open for 0% -> 0% of each run, Pallas kernels for 0% -> 0%
where the time goes in v1:
time: 103 us; the launch traced here: 102 us
  Pallas kernels  66.3 us (64%)
  matrix products  20.3 us (20%)
  other arithmetic  8.17 us (8%)
  local copies, waits for them, and re-layouts  6.64 us (6%)
    pallas_call x1, Pallas kernels, after_mixer(): pl.pallas_call(partial(tail_kernel, sp_count, tp_count, cap), out_shape=j...  55.5 us
    pallas_call x1, Pallas kernels, prefix(): pl.pallas_call(partial(share_kernel, size), out_shape=jax.ShapeDtypeStruc...  10.9 us
    dot_general x12, matrix products, square_product(): return jnp.einsum('hij,hjk->hik', first, second, precision=highest)  7.57 us
    dynamic_update_slice x4, other arithmetic, body(): lax.scan(advance, start, (block_trans.transpose(1, 0, 2, 3), block_state....  2.7 us

profile of v1, /device:TPU:0, one launch (start us, length us, event | category | flops | bytes accessed | tf_op | source)
XLA Modules:
  0.0 102.4 jit_solution(7020857330208987765)
XLA Ops:
  0.0 1.1 %reshape.115 = f32[4,32,4,64]{3,2,1,0:T(4,128)S(1)} reshape(f32[128,256]{1,0:T(8,128)} %param.22) | data formatting | bytes 262144 | tf_op jit(solution)/shard_map/reshape | solution.py:436
  1.1 0.9 convert_negate_fusion
  2.6 1.0 reshape.126
  3.7 0.9 add_divide_fusion
  5.1 0.6 convolution_multiply_fusion.3
  5.7 0.6 convolution_multiply_fusion.2
  6.3 0.4 fusion.65
  6.7 0.4 convolution_add_fusion.3
  7.1 0.4 fusion.66
  7.5 0.4 convolution_add_fusion.2
  8.3 0.4 convolution_add_fusion.1
  9.0 0.4 convolution_add_fusion
  9.4 0.6 convolution_multiply_fusion.1
  10.4 0.4 fusion.69
  10.8 0.4 fusion.70
  11.2 0.6 convolution_multiply_fusion
  12.1 0.4 fusion.71
  12.5 0.4 convolution_add_fusion.6
  13.0 1.1 %fusion.11 = f32[4,4,64,64]{3,2,0,1:T(8,128)S(1)} fusion(f32[4,4,32,64]{3,2,1,0:T(8,128)S(1)} %fusion.71, f32[4,4,64]{2,0,1:T(4,128)S(1)} %bitcast.181, f32[64,64]{1,0:T(8,128)S(1)} %fusion.57, f32[4,4,32,64]{3,2,1,0:T(8,128)S(1)} %get-tuple-element.120, f32[4,4,32,64]{3,2,1,0:T(8,128)S(1)} %reduce_window_sum.22, f32[4,4,64]{2,1,0:T(4,128)S(1)} %bitcast.177), kind=kOutput, calls=%fused_computation.19 | convolution fusion | flops 25362432 | bytes 679936 | tf_op jit(solution)/shard_map/hnsi,hnsj->hnij/dot_general | solution.py:521
  14.1 0.4 convolution_bitcast_fusion.2
  14.5 1.1 %fusion.12 = f32[4,4,64,64]{3,2,0,1:T(8,128)S(1)} fusion(f32[4,4,64,64]{3,2,0,1:T(8,128)S(1)} %convolution_bitcast_fusion.2, f32[4,4,32,64]{3,2,1,0:T(8,128)S(1)} %fusion.69, f32[4,4,32,64]{3,2,1,0:T(8,128)S(1)} %get-tuple-element.120, f32[4,4,32,64]{3,2,1,0:T(8,128)S(1)} %reduce_window_sum.22, f32[4,4,64]{2,1,0:T(4,128)S(1)} %bitcast.179), kind=kOutput, calls=%fused_computation.20 | convolution fusion | flops 25296896 | bytes 921600 | tf_op jit(solution)/shard_map/hnsi,hnsj->hnij/dot_general | solution.py:522
  15.6 6.8 %while.17 = (s32[]{:T(128)}, f32[4,64,64]{1,2,0:T(8,128)S(1)}, f32[4,64,64]{1,2,0:T(8,128)S(1)}, f32[4,4,64,64]{2,3,0,1:T(8,128)S(1)}, f32[4,4,64,64]{2,3,0,1:T(...) while((s32[]{:T(128)}, f32[4,64,64]{1,2,0:T(8,128)S(1)}, ...), condition=%wide.region_3.4_spmd.clone, body=%wide.region_2.3_spmd.clone.sunk | while | flops 25214980 | bytes 1835136 | solution.py:527
  15.8 0.7 bitcast_dynamic-update-slice_fusion.3
  16.5 0.4 convolution_bitcast_fusion.6
  17.0 0.4 fusion.121
  17.5 0.7 bitcast_dynamic-update-slice_fusion.3
  18.2 0.4 convolution_bitcast_fusion.6
  18.7 0.4 fusion.121
  19.1 0.7 bitcast_dynamic-update-slice_fusion.3
  19.8 0.4 convolution_bitcast_fusion.6
  20.3 0.4 fusion.121
  20.8 0.7 bitcast_dynamic-update-slice_fusion.3
  21.5 0.4 convolution_bitcast_fusion.6
  22.0 0.4 fusion.121
  22.5 1.6 %convolution_add_fusion.5 = f32[4,4,32,64]{3,2,1,0:T(8,128)S(1)} fusion(f32[4,4,32,64]{3,2,1,0:T(8,128)S(1)} %convolution_add_fusion.7, f32[4,4,32,64]{3,2,1,0:T(8,128)S(1)} %convolution_add_fusion.6, f32[4,4,64,64]{2,3,0,1:T(8,128)} %get-tuple-element.45), kind=kOutput, calls=%fused_computation.26 | convolution fusion | flops 25198592 | bytes 655360 | tf_op jit(solution)/shard_map/hntk,nhvk->hntv/dot_general | solution.py:531
  24.1 0.6 fusion.72
  24.9 0.7 pad_maximum_fusion.own_ref
  25.6 10.9 %shard_map.154 = bf16[4,4,64,128]{3,2,1,0:T(8,128)(2,1)} custom-call(bf16[4,64,128]{2,1,0:T(8,128)(2,1)} %pad_maximum_fusion.own_ref), custom_call_target="tpu_custom_call" | custom-call | tf_op jit(solution)/shard_map/pallas_call | solution.py:72
  36.5 1.1 %fusion.17 = f32[4,64,64]{2,1,0:T(8,128)S(1)} fusion(bf16[4,4,64,128]{3,2,1,0:T(8,128)(2,1)} %shard_map.154, pred[]{:T(512)S(6)} %gt.31), kind=kOutput, calls=%fused_computation.41 | convolution fusion | flops 12632064 | bytes 196609 | tf_op jit(solution)/shard_map/hij,hjk->hik/dot_general | solution.py:440
  37.6 1.1 %fusion.16 = f32[4,64,64]{2,1,0:T(8,128)S(1)} fusion(f32[4,64,64]{2,1,0:T(8,128)S(1)} %fusion.17, bf16[4,4,64,128]{3,2,1,0:T(8,128)(2,1)} %shard_map.154, pred[]{:T(512)S(6)} %gt.30), kind=kOutput, calls=%fused_computation.39 | convolution fusion | flops 12632064 | bytes 458753 | tf_op jit(solution)/shard_map/hij,hjk->hik/dot_general | solution.py:440
  38.7 1.1 %fusion.15 = f32[4,64,64]{2,1,0:T(8,128)S(1)} fusion(f32[4,64,64]{2,1,0:T(8,128)S(1)} %fusion.16, bf16[4,4,64,128]{3,2,1,0:T(8,128)(2,1)} %shard_map.154, pred[]{:T(512)S(6)} %gt.29), kind=kOutput, calls=%fused_computation.37 | convolution fusion | flops 12632064 | bytes 458753 | tf_op jit(solution)/shard_map/hij,hjk->hik/dot_general | solution.py:440
  39.9 1.1 %fusion.14 = f32[4,64,64,1]{2,1,3,0:T(8,128)S(1)} fusion(f32[4,64,64]{2,1,0:T(8,128)S(1)} %fusion.15, bf16[4,4,64,128]{3,2,1,0:T(8,128)(2,1)} %shard_map.154, pred[]{:T(512)S(6)} %gt.28), kind=kOutput, calls=%fused_computation.35 | convolution fusion | flops 12632064 | bytes 458753 | tf_op jit(solution)/shard_map/hij,hjk->hik/dot_general | solution.py:440
  41.0 0.5 fusion.64
  42.5 0.7 multiply_convert_fusion.gated_ref
  43.9 0.7 select_reduce_fusion
  44.6 0.7 copy.94
  45.3 55.5 %shard_map.155 = bf16[32,2048]{1,0:T(8,128)(2,1)} custom-call(bf16[128,256]{1,0:T(8,128)(2,1)} %multiply_convert_fusion.gated_ref, bf16[256,2048]{1,0:T(8,128)(2,1)} %out_weight_ref.1, bf16[32,2048]{1,0:T(8,128)(2,1)} %residual_ref.1, f32[1,2048]{1,0:T(1,128)} %bitcast.182, bf16[128,32]{1,0:T(8,128)(2,1)} %bitcast.180, ...), custom_call_target="tpu_custom_call" | custom-call | tf_op jit(solution)/shard_map/pallas_call | solution.py:393
  100.8 1.6 %copy.169 = bf16[32,2048]{1,0:T(8,128)(2,1)} copy(bf16[32,2048]{1,0:T(8,128)(2,1)} %shard_map.155) | data formatting | bytes 262144
  (68 shorter events, 5.2 us)
Async XLA Ops:
  0.0 4.9 %copy-start = (bf16[128,256]{1,0:T(8,128)(2,1)S(1)}, bf16[128,256]{1,0:T(8,128)(2,1)}, u32[]{:S(2)}) copy-start(bf16[128,256]{1,0:T(8,128)(2,1)} %param.18) | copy-start | bytes 196612
  6.3 3.7 %copy-start.1 = (bf16[128,256]{1,0:T(8,128)(2,1)S(1)}, bf16[128,256]{1,0:T(8,128)(2,1)}, u32[]{:S(2)}) copy-start(bf16[128,256]{1,0:T(8,128)(2,1)} %param.20) | copy-start | bytes 196612
  22.4 19.1 %copy-start.4 = (f32[256]{0:T(256)S(1)}, f32[256]{0:T(256)}, u32[]{:S(2)}) copy-start(f32[256]{0:T(256)} %param.25) | copy-start | bytes 3076
  22.4 20.0 %copy-start.2 = (bf16[128,256]{1,0:T(8,128)(2,1)S(1)}, bf16[128,256]{1,0:T(8,128)(2,1)}, u32[]{:S(2)}) copy-start(bf16[128,256]{1,0:T(8,128)(2,1)} %param.24) | copy-start | bytes 196612
  22.4 20.7 %copy-start.3 = (s32[32,2]{0,1:T(2,128)S(1)}, s32[32,2]{0,1:T(2,128)}, u32[]{:S(2)}) copy-start(s32[32,2]{0,1:T(2,128)} %param.29) | copy-start | bytes 772
  22.4 21.4 %copy-start.5 = (f32[32,2]{0,1:T(2,128)S(1)}, f32[32,2]{0,1:T(2,128)}, u32[]{:S(2)}) copy-start(f32[32,2]{0,1:T(2,128)} %param.30) | copy-start | bytes 772

commit v2 on v1

--- a/solution.py
+++ b/solution.py
@@ -19,12 +19,52 @@
 MESH = pl.DeviceIdType.MESH
 
 
-def share_kernel(size, own_ref, all_ref, send_sem, recv_sem):
+def exact(first, second):
+    return jnp.dot(first, second, precision=highest, preferred_element_type=jnp.float32)
+
+
+def exact_rows(first, second):
+    return lax.dot_general(
+        first,
+        second,
+        (((1,), (1,)), ((), ())),
+        precision=highest,
+        preferred_element_type=jnp.float32,
+    )
+
+
+def carry_kernel(
+    size,
+    trans_ref,
+    state_ref,
+    query_ref,
+    local_ref,
+    mixed_ref,
+    own_ref,
+    all_ref,
+    carried_ref,
+    incoming_ref,
+    send_sem,
+    recv_sem,
+):
     me = lax.axis_index("sp")
+    heads, blocks = trans_ref.shape[0], trans_ref.shape[1]
     barrier = pltpu.get_barrier_semaphore()
     for k in range(1, size):
         peer = lax.rem(me + k, size)
         pl.semaphore_signal(barrier, inc=1, device_id={"sp": peer}, device_id_type=MESH)
+
+    trans = [trans_ref[h, 0] for h in range(heads)]
+    state = [state_ref[h, 0] for h in range(heads)]
+    befores = []
+    for n in range(1, blocks):
+        befores.append((trans, state))
+        step = [trans_ref[h, n] for h in range(heads)]
+        trans = [exact(trans[h], step[h]) for h in range(heads)]
+        state = [exact(state[h], step[h]) + state_ref[h, n] for h in range(heads)]
+    for h in range(heads):
+        own_ref[h] = jnp.concatenate([trans[h], state[h]], axis=-1).astype(jnp.bfloat16)
+    incoming_ref[...] = jnp.zeros(incoming_ref.shape, jnp.float32)
     pl.semaphore_wait(barrier, size - 1)
 
     def transfer(slot, peer):
@@ -37,7 +77,7 @@
             device_id_type=MESH,
         )
 
-    def each(action):
+    def loop(action):
         def step(peer, carry):
             action(peer)
             return carry
@@ -49,43 +89,53 @@
         def _():
             transfer(me, peer).start()
 
-        @pl.when(peer >= me)
-        def _():
-            all_ref[peer] = jnp.zeros(own_ref.shape, own_ref.dtype)
+    def receive(peer):
+        @pl.when(peer < me)
+        def _():
+            transfer(peer, peer).wait_recv()
+            for h in range(heads):
+                item = all_ref[peer, h].astype(jnp.float32)
+                incoming_ref[h] = exact(incoming_ref[h], item[:, :HEAD]) + item[:, HEAD:]
 
     def finish(peer):
         @pl.when(peer > me)
         def _():
             transfer(me, peer).wait_send()
 
-        @pl.when(peer < me)
-        def _():
-            transfer(peer, peer).wait_recv()
-
-    each(send)
-    each(finish)
-
-
-def prefix(x, axis, combine, identity):
-    size, index = (lax.axis_size(axis), lax.axis_index(axis))
-    own = jnp.concatenate([part.astype(jnp.bfloat16) for part in x], axis=-1)
-    everything = pl.pallas_call(
-        partial(share_kernel, size),
-        out_shape=jax.ShapeDtypeStruct((size,) + own.shape, own.dtype),
-        in_specs=[pl.BlockSpec(memory_space=pltpu.VMEM)],
-        out_specs=pl.BlockSpec(memory_space=pltpu.VMEM),
-        scratch_shapes=[pltpu.SemaphoreType.DMA((size,)), pltpu.SemaphoreType.DMA((size,))],
+    loop(send)
+    for h in range(heads):
+        carried_ref[h, 0] = query_ref[h, 0]
+        mixed_ref[h, 0] = local_ref[h, 0]
+        for n in range(1, blocks):
+            trans, state = befores[n - 1]
+            carried_ref[h, n] = exact_rows(query_ref[h, n], trans[h])
+            mixed_ref[h, n] = local_ref[h, n] + exact_rows(query_ref[h, n], state[h])
+    loop(receive)
+    for h in range(heads):
+        for n in range(blocks):
+            mixed_ref[h, n] = mixed_ref[h, n] + exact_rows(carried_ref[h, n], incoming_ref[h])
+    loop(finish)
+
+
+def carry(trans, state, query, local):
+    size = lax.axis_size("sp")
+    heads = trans.shape[0]
+    vmem = pl.BlockSpec(memory_space=pltpu.VMEM)
+    return pl.pallas_call(
+        partial(carry_kernel, size),
+        out_shape=jax.ShapeDtypeStruct(local.shape, jnp.float32),
+        in_specs=[vmem] * 4,
+        out_specs=vmem,
+        scratch_shapes=[
+            pltpu.VMEM((heads, HEAD, 2 * HEAD), jnp.bfloat16),
+            pltpu.VMEM((size, heads, HEAD, 2 * HEAD), jnp.bfloat16),
+            pltpu.VMEM(query.shape, jnp.float32),
+            pltpu.VMEM((heads, HEAD, HEAD), jnp.float32),
+            pltpu.SemaphoreType.DMA((size,)),
+            pltpu.SemaphoreType.DMA((size,)),
+        ],
         compiler_params=pltpu.CompilerParams(collective_id=1, has_side_effects=True),
-    )(own)
-    before = identity
-    for k in range(size):
-        item = (
-            everything[k, :, :, :HEAD].astype(jnp.float32),
-            everything[k, :, :, HEAD:].astype(jnp.float32),
-        )
-        new = combine(before, item)
-        before = jax.tree.map(lambda p, q: jnp.where(k < index, p, q), new, before)
-    return before
+    )(trans, state, query, local)
 
 
 def tail_kernel(
@@ -434,25 +484,6 @@
     blocks = array.shape[0] // BLK
     heads_here = array.shape[1] // HEAD
     return array.astype(jnp.float32).reshape(blocks, BLK, heads_here, HEAD).transpose(2, 0, 1, 3)
-
-
-def square_product(first, second):
-    return jnp.einsum("hij,hjk->hik", first, second, precision=highest)
-
-
-def join_later(earlier, later):
-    trans_a, state_a = earlier
-    trans_b, state_b = later
-    return (square_product(trans_a, trans_b), square_product(state_a, trans_b) + state_b)
-
-
-def advance(carry, item):
-    prod_now, state_now = carry
-    trans_here, local_here = item
-    return (
-        (square_product(prod_now, trans_here), square_product(state_now, trans_here) + local_here),
-        (prod_now, state_now),
-    )
 
 
 def body(
@@ -520,17 +551,7 @@
     eye_head = jnp.eye(HEAD, dtype=jnp.float32)
     block_trans = eye_head * jnp.exp(final_log) + outer_sum(from_start, insert_tail)
     block_state = outer_sum(from_local, insert_tail) + outer_sum(valued, key_tail)
-    start = (
-        jnp.broadcast_to(eye_head, (heads_here, HEAD, HEAD)),
-        jnp.zeros((heads_here, HEAD, HEAD), jnp.float32),
-    )
-    (device_trans, device_state), (prefix_trans, prefix_state) = lax.scan(
-        advance, start, (block_trans.transpose(1, 0, 2, 3), block_state.transpose(1, 0, 2, 3))
-    )
-    carried_query = jnp.einsum("hntk,nhjk->hntj", query_map, prefix_trans, precision=highest)
-    own_out = local_out + jnp.einsum("hntk,nhvk->hntv", query_map, prefix_state, precision=highest)
-    incoming = prefix((device_trans, device_state), "sp", join_later, start)
-    mixed = own_out + jnp.einsum("hntk,hvk->hntv", carried_query, incoming[1], precision=highest)
+    mixed = carry(block_trans, block_state, query_map, local_out)
     centre = mixed - jnp.mean(mixed, axis=-1, keepdims=True)
     spread = jnp.mean(centre * centre, axis=-1, keepdims=True)
     normed = centre * lax.rsqrt(spread + 0.00064) * head_norm_gain.reshape(heads_here, 1, 1, HEAD)

time: 103 us -> 95.5 us (0.927)
  matrix products: 20.3 us -> 13.1 us
  Pallas kernels: 66.3 us -> 68.1 us
    dot_general x15 -> x0, matrix products: 10.3 us -> none  [the longest x12 7.57 us: square_product(): return jnp.einsum('hij,hjk->hik', first, second, precision=highest)]
    dynamic_update_slice x4 -> x0, other arithmetic: 2.7 us -> none  [body(): lax.scan(advance, start, (block_trans.transpose(1, 0, 2, 3), block_state....]
    pallas_call x1, Pallas kernels: 55.5 us -> 56.8 us  [after_mixer(): pl.pallas_call(partial(tail_kernel, sp_count, tp_count, cap), out_shape=j...]
    transpose x0 -> x1, other arithmetic: none -> 1.15 us  [body(): normed = normed.transpose(1, 2, 0, 3).reshape(length_here, width_here)]
    reduce_sum x0 -> x1, other arithmetic: none -> 1.1 us  [body(): centre = mixed - jnp.mean(mixed, axis=-1, keepdims=True)]
where the time goes in v2:
time: 95.5 us; the launch traced here: 95.1 us
  Pallas kernels  68.1 us (71%)
  matrix products  13.1 us (14%)
  other arithmetic  7.71 us (8%)
  local copies, waits for them, and re-layouts  5.79 us (6%)
    pallas_call x1, Pallas kernels, after_mixer(): pl.pallas_call(partial(tail_kernel, sp_count, tp_count, cap), out_shape=j...  56.8 us
    pallas_call x1, Pallas kernels, carry(): pl.pallas_call(partial(carry_kernel, size), out_shape=jax.ShapeDtypeStruc...  11.4 us

profile of v2, /device:TPU:0, one launch (start us, length us, event | category | flops | bytes accessed | tf_op | source)
XLA Modules:
  0.0 95.1 jit_solution(13261020008139476332)
XLA Ops:
  0.0 0.8 convert_negate_fusion
  0.9 0.2 neg.35
  1.0 1.1 %reshape.106 = f32[4,32,4,64]{3,2,1,0:T(4,128)S(1)} reshape(f32[128,256]{1,0:T(8,128)} %param.20) | data formatting | bytes 262144 | tf_op jit(solution)/shard_map/reshape | solution.py:486
  2.1 0.2 fusion.5
  2.3 0.2 reduce_window_sum.22
  2.5 1.0 %reshape.113 = f32[4,32,4,64]{3,2,1,0:T(4,128)S(1)} reshape(bf16[128,256]{1,0:T(8,128)(2,1)} %param.17) | data formatting | bytes 196608 | tf_op jit(solution)/shard_map/transpose | solution.py:486
  3.5 0.2 fusion.6
  3.7 0.9 add_divide_fusion
  4.6 0.2 reshape.112
  4.7 0.1 bitcast_multiply_fusion.1
  4.9 0.6 convolution_multiply_fusion.3
  5.5 0.4 fusion.35
  5.9 0.4 convolution_add_fusion.4
  6.3 0.4 fusion.36
  6.7 0.4 convolution_add_fusion.3
  7.1 0.4 fusion.37
  7.5 0.4 convolution_add_fusion.2
  7.9 0.4 fusion.38
  8.3 0.4 convolution_add_fusion.1
  8.7 0.6 convolution_multiply_fusion.2
  9.2 0.1 reshape.108
  9.4 0.3 fusion.17
  9.6 0.4 fusion.40
  10.0 0.2 reshape.114
  10.2 0.6 convolution_multiply_fusion.1
  10.8 0.4 fusion.41
  11.2 0.6 convolution_multiply_fusion
  11.8 1.0 %convolution_add_fusion.5.local_ref = f32[4,4,32,64]{3,2,1,0:T(8,128)} fusion(f32[4,4,32,64]{3,2,1,0:T(8,128)S(1)} %fusion.41, f32[4,4,32,32]{3,2,1,0:T(8,128)S(1)} %convolution_multiply_fusion, bf16[4,32,4,64]{3,2,1,0:T(4,128)(2,1)S(1)} %reshape.108), kind=kOutput, calls=%fused_computation.7 | convolution fusion | flops 12615680 | bytes 393216 | tf_op jit(solution)/shard_map/hnts,hnsc->hntc/dot_general | solution.py:547
  12.8 0.4 fusion.39
  13.2 1.1 %convolution_add_fusion.6.query_ref = f32[4,4,32,64]{3,2,1,0:T(8,128)} fusion(f32[4,4,32,32]{3,2,1,0:T(8,128)S(1)} %convolution_multiply_fusion.1, f32[4,4,32,64]{3,2,1,0:T(8,128)S(1)} %fusion.39, f32[4,4,32,64]{3,2,1,0:T(8,128)S(1)} %reduce_window_sum.22, f32[4,32,4,64]{3,2,1,0:T(4,128)S(1)} %reshape.114), kind=kOutput, calls=%fused_computation.9 | convolution fusion | flops 12648448 | bytes 589824 | tf_op jit(solution)/shard_map/hnts,hnsc->hntc/dot_general | solution.py:546
  14.3 1.1 %fusion.26 = f32[4,4,64,64]{3,2,1,0:T(8,128)S(1)} fusion(f32[4,4,32,64]{3,2,1,0:T(8,128)S(1)} %fusion.40, f32[4,4,32,64]{3,2,1,0:T(8,128)S(1)} %get-tuple-element.7, f32[4,4,32,64]{3,2,1,0:T(8,128)S(1)} %reduce_window_sum.22, f32[4,4,64]{2,1,0:T(4,128)S(1)} %bitcast.86), kind=kOutput, calls=%fused_computation.53 | convolution fusion | flops 25231360 | bytes 659456 | tf_op jit(solution)/shard_map/hnsi,hnsj->hnij/dot_general | solution.py:553
  15.4 1.2 %fusion.state_ref = f32[4,4,64,64]{3,2,1,0:T(8,128)} fusion(f32[4,4,64,64]{3,2,1,0:T(8,128)S(1)} %fusion.26, f32[4,4,32,64]{3,2,1,0:T(8,128)S(1)} %reduce_window_sum.22, f32[4,32,4,64]{3,2,1,0:T(4,128)S(1)} %reshape.113, f32[4,4,64]{2,1,0:T(4,128)S(1)} %bitcast.87, bf16[4,32,4,64]{3,2,1,0:T(4,128)(2,1)S(1)} %reshape.108), kind=kOutput, calls=%fused_computation.1 | convolution fusion | flops 25296896 | bytes 856064 | tf_op jit(solution)/shard_map/hnsi,hnsj->hnij/dot_general | solution.py:553
  16.7 1.9 %convolution_add_fusion.trans_ref = f32[4,4,64,64]{3,2,1,0:T(8,128)} fusion(f32[4,4,32,64]{3,2,1,0:T(8,128)S(1)} %fusion.39, f32[4,4,64]{2,1,0:T(4,128)S(1)} %bitcast.90, f32[64,64]{1,0:T(8,128)S(1)} %fusion.30, f32[4,4,32,64]{3,2,1,0:T(8,128)S(1)} %get-tuple-element.7, f32[4,4,32,64]{3,2,1,0:T(8,128)S(1)} %reduce_window_sum.22, f32[4,4,64]{2,1,0:T(4,128)S(1)} %bitcast.88), kind=kOutput, calls=%fused_computation.2 | convolution fusion | flops 25362432 | bytes 679936 | tf_op jit(solution)/shard_map/hnsi,hnsj->hnij/dot_general | solution.py:552
  18.6 11.4 %shard_map.154 = f32[4,4,32,64]{3,2,1,0:T(8,128)} custom-call(f32[4,4,64,64]{3,2,1,0:T(8,128)} %convolution_add_fusion.trans_ref, f32[4,4,64,64]{3,2,1,0:T(8,128)} %fusion.state_ref, f32[4,4,32,64]{3,2,1,0:T(8,128)} %convolution_add_fusion.6.query_ref, f32[4,4,32,64]{3,2,1,0:T(8,128)} %convolution_add_fusion.5.local_ref), custom_call_target="tpu_custom_call" | custom-call | tf_op jit(solution)/shard_map/pallas_call | solution.py:124
  29.9 1.1 %reduce_sum.57 = f32[4,4,32]{2,1,0:T(4,128)S(1)} reduce(f32[4,4,32,64]{3,2,1,0:T(8,128)} %shard_map.154, f32[]{:T(128)} %constant.11.clone.1), dimensions={3}, to_apply=%region_2.3 | reduce | flops 32256 | bytes 133124 | tf_op jit(solution)/shard_map/reduce_sum | solution.py:555
  31.0 1.2 %multiply_reduce_fusion = f32[4,4,32]{2,1,0:T(4,128)S(1)} fusion(f32[4,4,32,64]{3,2,1,0:T(8,128)} %shard_map.154, f32[4,4,32]{2,1,0:T(4,128)S(1)} %broadcast_multiply_fusion), kind=kLoop, calls=%fused_computation.33 | loop fusion | flops 97792 | bytes 135168 | tf_op jit(solution)/shard_map/reduce_sum | solution.py:556
  32.4 1.1 %multiply_bitcast_fusion = f32[4,32,4,64]{3,1,0,2:T(8,128)S(1)} fusion(f32[4,4,32,64]{3,2,1,0:T(8,128)} %shard_map.154, f32[4,64]{1,0:T(4,128)S(1)} %mul.147, f32[4,4,32]{2,1,0:T(4,128)S(1)} %add_rsqrt_fusion, f32[4,4,32]{2,1,0:T(4,128)S(1)} %broadcast_multiply_fusion), kind=kLoop, calls=%fused_computation.32 | loop fusion | flops 98304 | bytes 267264 | tf_op jit(solution)/shard_map/transpose | solution.py:558
  33.5 0.2 copy.57
  33.7 0.2 reshape.110
  33.9 0.7 multiply_convert_fusion.gated_ref
  34.7 0.1 eq.45
  34.8 0.1 reduce_window_sum.23
  34.9 0.2 select_reduce_fusion.1
  35.1 0.1 reduce_sum.60
  35.3 0.7 select_reduce_fusion
  36.0 0.7 copy.60
  36.7 56.8 %shard_map.155 = bf16[32,2048]{1,0:T(8,128)(2,1)} custom-call(bf16[128,256]{1,0:T(8,128)(2,1)} %multiply_convert_fusion.gated_ref, bf16[256,2048]{1,0:T(8,128)(2,1)} %out_weight_ref.1, bf16[32,2048]{1,0:T(8,128)(2,1)} %residual_ref.1, f32[1,2048]{1,0:T(1,128)} %bitcast.91, bf16[128,32]{1,0:T(8,128)(2,1)} %bitcast.89, ...), custom_call_target="tpu_custom_call" | custom-call | tf_op jit(solution)/shard_map/pallas_call | solution.py:443
  93.5 1.6 %copy.93 = bf16[32,2048]{1,0:T(8,128)(2,1)} copy(bf16[32,2048]{1,0:T(8,128)(2,1)} %shard_map.155) | data formatting | bytes 262144
  (25 shorter events, 0.4 us)
Async XLA Ops:
  5.5 3.8 %copy-start = (bf16[128,256]{1,0:T(8,128)(2,1)S(1)}, bf16[128,256]{1,0:T(8,128)(2,1)}, u32[]{:S(2)}) copy-start(bf16[128,256]{1,0:T(8,128)(2,1)} %param.18) | copy-start | bytes 196612
  6.3 3.7 %copy-start.1 = (bf16[128,256]{1,0:T(8,128)(2,1)S(1)}, bf16[128,256]{1,0:T(8,128)(2,1)}, u32[]{:S(2)}) copy-start(bf16[128,256]{1,0:T(8,128)(2,1)} %param.16) | copy-start | bytes 196612
  14.3 18.0 %copy-start.4 = (f32[256]{0:T(256)S(1)}, f32[256]{0:T(256)}, u32[]{:S(2)}) copy-start(f32[256]{0:T(256)} %param.23) | copy-start | bytes 3076
  15.4 18.5 %copy-start.2 = (bf16[128,256]{1,0:T(8,128)(2,1)S(1)}, bf16[128,256]{1,0:T(8,128)(2,1)}, u32[]{:S(2)}) copy-start(bf16[128,256]{1,0:T(8,128)(2,1)} %param.22) | copy-start | bytes 196612
  15.4 19.2 %copy-start.3 = (s32[32,2]{0,1:T(2,128)S(1)}, s32[32,2]{0,1:T(2,128)}, u32[]{:S(2)}) copy-start(s32[32,2]{0,1:T(2,128)} %param.27) | copy-start | bytes 772
  15.4 19.9 %copy-start.5 = (f32[32,2]{0,1:T(2,128)S(1)}, f32[32,2]{0,1:T(2,128)}, u32[]{:S(2)}) copy-start(f32[32,2]{0,1:T(2,128)} %param.28) | copy-start | bytes 772

commit v3 on v2

--- a/solution.py
+++ b/solution.py
@@ -371,18 +371,18 @@
             final_copy(s, sp).start()
 
     fan_first(0)
+    fan_second(0)
     if sp_count > 1:
         fan_first(1)
-    fan_second(0)
 
     def turn(i):
+        @pl.when(i < sp_count)
+        def _():
+            compute(i)
+
         @pl.when(i + 1 < sp_count)
         def _():
             fan_second(i + 1)
-
-        @pl.when(i < sp_count)
-        def _():
-            compute(i)
 
         @pl.when(i + 2 < sp_count)
         def _():

time: 95.5 us -> 91.4 us (0.957)
  Pallas kernels: 68.1 us -> 64.1 us
    pallas_call x1, Pallas kernels: 56.8 us -> 52.7 us  [after_mixer(): pl.pallas_call(partial(tail_kernel, sp_count, tp_count, cap), out_shape=j...]
where the time goes in v3:
time: 91.4 us; the launch traced here: 91 us
  Pallas kernels  64.1 us (70%)
  matrix products  13.1 us (14%)
  other arithmetic  7.71 us (8%)
  local copies, waits for them, and re-layouts  5.79 us (6%)
    pallas_call x1, Pallas kernels, after_mixer(): pl.pallas_call(partial(tail_kernel, sp_count, tp_count, cap), out_shape=j...  52.7 us
    pallas_call x1, Pallas kernels, carry(): pl.pallas_call(partial(carry_kernel, size), out_shape=jax.ShapeDtypeStruc...  11.4 us
    dot_general x1, matrix products, body(): outer_sum(from_start, insert_tail)  1.86 us

profile of v3, /device:TPU:0, one launch (start us, length us, event | category | flops | bytes accessed | tf_op | source)
XLA Modules:
  0.0 91.0 jit_solution(14515683561388568259)
XLA Ops:
  0.0 0.8 convert_negate_fusion
  0.9 0.2 neg.35
  1.0 1.1 %reshape.106 = f32[4,32,4,64]{3,2,1,0:T(4,128)S(1)} reshape(f32[128,256]{1,0:T(8,128)} %param.20) | data formatting | bytes 262144 | tf_op jit(solution)/shard_map/reshape | solution.py:486
  2.1 0.2 fusion.5
  2.3 0.2 reduce_window_sum.22
  2.5 1.0 %reshape.113 = f32[4,32,4,64]{3,2,1,0:T(4,128)S(1)} reshape(bf16[128,256]{1,0:T(8,128)(2,1)} %param.17) | data formatting | bytes 196608 | tf_op jit(solution)/shard_map/transpose | solution.py:486
  3.5 0.2 fusion.6
  3.7 0.9 add_divide_fusion
  4.6 0.2 reshape.112
  4.7 0.1 bitcast_multiply_fusion.1
  4.9 0.6 convolution_multiply_fusion.3
  5.5 0.4 fusion.35
  5.9 0.4 convolution_add_fusion.4
  6.3 0.4 fusion.36
  6.7 0.4 convolution_add_fusion.3
  7.1 0.4 fusion.37
  7.5 0.4 convolution_add_fusion.2
  7.9 0.4 fusion.38
  8.3 0.4 convolution_add_fusion.1
  8.7 0.6 convolution_multiply_fusion.2
  9.2 0.1 reshape.108
  9.4 0.3 fusion.17
  9.6 0.4 fusion.40
  10.0 0.2 reshape.114
  10.2 0.6 convolution_multiply_fusion.1
  10.8 0.4 fusion.41
  11.2 0.6 convolution_multiply_fusion
  11.8 1.0 %convolution_add_fusion.5.local_ref = f32[4,4,32,64]{3,2,1,0:T(8,128)} fusion(f32[4,4,32,64]{3,2,1,0:T(8,128)S(1)} %fusion.41, f32[4,4,32,32]{3,2,1,0:T(8,128)S(1)} %convolution_multiply_fusion, bf16[4,32,4,64]{3,2,1,0:T(4,128)(2,1)S(1)} %reshape.108), kind=kOutput, calls=%fused_computation.7 | convolution fusion | flops 12615680 | bytes 393216 | tf_op jit(solution)/shard_map/hnts,hnsc->hntc/dot_general | solution.py:547
  12.8 0.4 fusion.39
  13.2 1.1 %convolution_add_fusion.6.query_ref = f32[4,4,32,64]{3,2,1,0:T(8,128)} fusion(f32[4,4,32,32]{3,2,1,0:T(8,128)S(1)} %convolution_multiply_fusion.1, f32[4,4,32,64]{3,2,1,0:T(8,128)S(1)} %fusion.39, f32[4,4,32,64]{3,2,1,0:T(8,128)S(1)} %reduce_window_sum.22, f32[4,32,4,64]{3,2,1,0:T(4,128)S(1)} %reshape.114), kind=kOutput, calls=%fused_computation.9 | convolution fusion | flops 12648448 | bytes 589824 | tf_op jit(solution)/shard_map/hnts,hnsc->hntc/dot_general | solution.py:546
  14.3 1.1 %fusion.26 = f32[4,4,64,64]{3,2,1,0:T(8,128)S(1)} fusion(f32[4,4,32,64]{3,2,1,0:T(8,128)S(1)} %fusion.40, f32[4,4,32,64]{3,2,1,0:T(8,128)S(1)} %get-tuple-element.7, f32[4,4,32,64]{3,2,1,0:T(8,128)S(1)} %reduce_window_sum.22, f32[4,4,64]{2,1,0:T(4,128)S(1)} %bitcast.86), kind=kOutput, calls=%fused_computation.53 | convolution fusion | flops 25231360 | bytes 659456 | tf_op jit(solution)/shard_map/hnsi,hnsj->hnij/dot_general | solution.py:553
  15.4 1.2 %fusion.state_ref = f32[4,4,64,64]{3,2,1,0:T(8,128)} fusion(f32[4,4,64,64]{3,2,1,0:T(8,128)S(1)} %fusion.26, f32[4,4,32,64]{3,2,1,0:T(8,128)S(1)} %reduce_window_sum.22, f32[4,32,4,64]{3,2,1,0:T(4,128)S(1)} %reshape.113, f32[4,4,64]{2,1,0:T(4,128)S(1)} %bitcast.87, bf16[4,32,4,64]{3,2,1,0:T(4,128)(2,1)S(1)} %reshape.108), kind=kOutput, calls=%fused_computation.1 | convolution fusion | flops 25296896 | bytes 856064 | tf_op jit(solution)/shard_map/hnsi,hnsj->hnij/dot_general | solution.py:553
  16.7 1.9 %convolution_add_fusion.trans_ref = f32[4,4,64,64]{3,2,1,0:T(8,128)} fusion(f32[4,4,32,64]{3,2,1,0:T(8,128)S(1)} %fusion.39, f32[4,4,64]{2,1,0:T(4,128)S(1)} %bitcast.90, f32[64,64]{1,0:T(8,128)S(1)} %fusion.30, f32[4,4,32,64]{3,2,1,0:T(8,128)S(1)} %get-tuple-element.7, f32[4,4,32,64]{3,2,1,0:T(8,128)S(1)} %reduce_window_sum.22, f32[4,4,64]{2,1,0:T(4,128)S(1)} %bitcast.88), kind=kOutput, calls=%fused_computation.2 | convolution fusion | flops 25362432 | bytes 679936 | tf_op jit(solution)/shard_map/hnsi,hnsj->hnij/dot_general | solution.py:552
  18.6 11.4 %shard_map.154 = f32[4,4,32,64]{3,2,1,0:T(8,128)} custom-call(f32[4,4,64,64]{3,2,1,0:T(8,128)} %convolution_add_fusion.trans_ref, f32[4,4,64,64]{3,2,1,0:T(8,128)} %fusion.state_ref, f32[4,4,32,64]{3,2,1,0:T(8,128)} %convolution_add_fusion.6.query_ref, f32[4,4,32,64]{3,2,1,0:T(8,128)} %convolution_add_fusion.5.local_ref), custom_call_target="tpu_custom_call" | custom-call | tf_op jit(solution)/shard_map/pallas_call | solution.py:124
  29.9 1.1 %reduce_sum.57 = f32[4,4,32]{2,1,0:T(4,128)S(1)} reduce(f32[4,4,32,64]{3,2,1,0:T(8,128)} %shard_map.154, f32[]{:T(128)} %constant.11.clone.1), dimensions={3}, to_apply=%region_2.3 | reduce | flops 32256 | bytes 133124 | tf_op jit(solution)/shard_map/reduce_sum | solution.py:555
  31.0 1.2 %multiply_reduce_fusion = f32[4,4,32]{2,1,0:T(4,128)S(1)} fusion(f32[4,4,32,64]{3,2,1,0:T(8,128)} %shard_map.154, f32[4,4,32]{2,1,0:T(4,128)S(1)} %broadcast_multiply_fusion), kind=kLoop, calls=%fused_computation.33 | loop fusion | flops 97792 | bytes 135168 | tf_op jit(solution)/shard_map/reduce_sum | solution.py:556
  32.4 1.1 %multiply_bitcast_fusion = f32[4,32,4,64]{3,1,0,2:T(8,128)S(1)} fusion(f32[4,4,32,64]{3,2,1,0:T(8,128)} %shard_map.154, f32[4,64]{1,0:T(4,128)S(1)} %mul.147, f32[4,4,32]{2,1,0:T(4,128)S(1)} %add_rsqrt_fusion, f32[4,4,32]{2,1,0:T(4,128)S(1)} %broadcast_multiply_fusion), kind=kLoop, calls=%fused_computation.32 | loop fusion | flops 98304 | bytes 267264 | tf_op jit(solution)/shard_map/transpose | solution.py:558
  33.5 0.2 copy.57
  33.7 0.2 reshape.110
  33.9 0.7 multiply_convert_fusion.gated_ref
  34.7 0.1 eq.45
  34.8 0.1 reduce_window_sum.23
  34.9 0.2 select_reduce_fusion.1
  35.1 0.1 reduce_sum.60
  35.3 0.7 select_reduce_fusion
  36.0 0.7 copy.60
  36.7 52.7 %shard_map.155 = bf16[32,2048]{1,0:T(8,128)(2,1)} custom-call(bf16[128,256]{1,0:T(8,128)(2,1)} %multiply_convert_fusion.gated_ref, bf16[256,2048]{1,0:T(8,128)(2,1)} %out_weight_ref.1, bf16[32,2048]{1,0:T(8,128)(2,1)} %residual_ref.1, f32[1,2048]{1,0:T(1,128)} %bitcast.91, bf16[128,32]{1,0:T(8,128)(2,1)} %bitcast.89, ...), custom_call_target="tpu_custom_call" | custom-call | tf_op jit(solution)/shard_map/pallas_call | solution.py:443
  89.4 1.6 %copy.93 = bf16[32,2048]{1,0:T(8,128)(2,1)} copy(bf16[32,2048]{1,0:T(8,128)(2,1)} %shard_map.155) | data formatting | bytes 262144
  (25 shorter events, 0.4 us)
Async XLA Ops:
  5.5 3.8 %copy-start = (bf16[128,256]{1,0:T(8,128)(2,1)S(1)}, bf16[128,256]{1,0:T(8,128)(2,1)}, u32[]{:S(2)}) copy-start(bf16[128,256]{1,0:T(8,128)(2,1)} %param.18) | copy-start | bytes 196612
  6.3 3.7 %copy-start.1 = (bf16[128,256]{1,0:T(8,128)(2,1)S(1)}, bf16[128,256]{1,0:T(8,128)(2,1)}, u32[]{:S(2)}) copy-start(bf16[128,256]{1,0:T(8,128)(2,1)} %param.16) | copy-start | bytes 196612
  14.3 18.0 %copy-start.4 = (f32[256]{0:T(256)S(1)}, f32[256]{0:T(256)}, u32[]{:S(2)}) copy-start(f32[256]{0:T(256)} %param.23) | copy-start | bytes 3076
  15.4 18.5 %copy-start.2 = (bf16[128,256]{1,0:T(8,128)(2,1)S(1)}, bf16[128,256]{1,0:T(8,128)(2,1)}, u32[]{:S(2)}) copy-start(bf16[128,256]{1,0:T(8,128)(2,1)} %param.22) | copy-start | bytes 196612
  15.4 19.2 %copy-start.3 = (s32[32,2]{0,1:T(2,128)S(1)}, s32[32,2]{0,1:T(2,128)}, u32[]{:S(2)}) copy-start(s32[32,2]{0,1:T(2,128)} %param.27) | copy-start | bytes 772
  15.4 19.9 %copy-start.5 = (f32[32,2]{0,1:T(2,128)S(1)}, f32[32,2]{0,1:T(2,128)}, u32[]{:S(2)}) copy-start(f32[32,2]{0,1:T(2,128)} %param.28) | copy-start | bytes 772
